TPU v7x, 512 devices: a whole 4x4x16 slice. The times are simulated.
512 devices in a mesh: dp: 4 (over x), kv: 64 (over z, y), tp: 2 (over core).
Axes of the slice: x: 4, y: 4, z: 16, core: 2. Of those that a mesh axis runs over, the one named last changes fastest.
Arguments:
- tokens: bfloat16 [16, 24, 2048], P('dp'), may hold values from -6 to 6
- norm_gain: bfloat16 [2048], replicated, may hold values from 0.099609375 to 1.8984375
- w_query: bfloat16 [2048, 1024], P('kv', 'tp'), may hold values from -0.125 to 0.125
- w_key: bfloat16 [2048, 1024], P('kv', 'tp'), may hold values from -0.03125 to 0.03125
- w_value: bfloat16 [2048, 1024], P('kv', 'tp'), may hold values from -0.03125 to 0.03125
- w_forget: bfloat16 [2048, 16], P('kv', 'tp'), may hold values from -0.125 to 0.125
- forget_bias: float32 [16], P('tp'), may hold values from 0 to 4
- head_gain: bfloat16 [1024], P('tp'), may hold values from 0.099609375 to 1.8984375
- w_out: bfloat16 [1024, 2048], P('tp', 'kv'), may hold values from -0.1875 to 0.1875
- cache_keys: bfloat16 [16, 16384, 1024], P('dp', 'kv', 'tp'), may hold values from -480 to 480
- cache_values: bfloat16 [16, 16384, 1024], P('dp', 'kv', 'tp'), may hold values from -1.5 to 1.5
- cache_gates: float32 [16, 16, 16384], P('dp', 'tp', 'kv'), may hold values from -2048 to 0, as said below
- lengths: int32 [16], P('dp'), may hold values from 8192 to 16335
- accepted: int32 [16], P('dp'), may hold values from 0 to 23
- parents: int32 [16, 24], P('dp'), may hold values from -1 to 22, as said below
Outputs:
- mixed: float32 [16, 24, 2048], P('dp', None, ('kv', 'tp'))
- keys_out: bfloat16 [16, 16384, 1024], P('dp', 'kv', 'tp')
- values_out: bfloat16 [16, 16384, 1024], P('dp', 'kv', 'tp')
- gates_out: float32 [16, 16, 16384], P('dp', 'tp', 'kv')
Inputs may be any that keep to these rules, and one draw needn't show every extreme that they name: parents[b, 0] = -1 and 0 <= parents[b, j] < j for every later proposal j. `cache_gates`: nonincreasing along the positions of each sequence and head.
All inputs are finite; a program needn't handle non-finite values.
Results may differ from a plain program's by a relative error of at most 0.008.
Values may be sent and summed in bfloat16 or wider, within the bound.
No kernel may reach another device: no remote copies, remote signals or barrier semaphores. Data moves between devices by JAX's collectives and lax.ppermute only.
A program may use at most 64 MiB of HBM per device.

v0:
```python
import jax
import jax.numpy as jnp
from jax import lax
from jax.sharding import Mesh
from jax.sharding import PartitionSpec as P

KV = ("kv_0", "kv_1")
KV_TP = ("kv_0", "kv_1", "tp")
NEG_LARGE = -1e30
EPSILON = 1e-06


def in_one_piece(arrays, axis, dim, along):
    widths = [a.shape[along] for a in arrays]
    both = jnp.concatenate(arrays, axis=along)
    whole = lax.all_gather(both, axis, axis=dim, tiled=True)
    return tuple(jnp.split(whole, [sum(widths[:k]) for k in range(1, len(widths))], axis=along))


def one_axis_at_a_time(array, axes):
    for axis in axes:
        array = lax.psum(array, axis)
    return array


def collected_together(array, axis):
    leaves = jax.tree.leaves(array)
    sequence = sorted(range(len(leaves)), key=lambda k: -leaves[k].size)
    width = (1, *leaves[sequence[0]].shape)[-1]
    lines = [
        jnp.pad(leaves[k].reshape(-1), (0, -leaves[k].size % width)).reshape(-1, width)
        for k in sequence
    ]
    both, at, found = (lax.all_gather(jnp.concatenate(lines), axis), 0, {})
    for k, line in zip(sequence, lines):
        piece = both[:, at : at + len(line)].reshape(len(both), -1)
        found[k] = piece[:, : leaves[k].size].reshape(-1, *leaves[k].shape)
        at += len(line)
    numbers = iter(range(len(leaves)))
    return jax.tree.map(lambda _: found[next(numbers)], array)


def merged_by_axis(array, axes, combine):
    for axis in axes:
        pieces = collected_together(array, axis)
        array = jax.tree.map(lambda part: part[0], pieces)
        for k in range(1, lax.axis_size(axis)):
            array = combine(array, jax.tree.map(lambda part: part[k], pieces))
    return array


def in_blocks(array, dim, peers):
    before, after = (array.shape[:dim], array.shape[dim + 1 :])
    return jnp.moveaxis(array.reshape(*before, peers, -1, *after), dim, 0)


def sent_and_summed(array, axis, dim):
    pieces = in_blocks(array, dim, lax.axis_size(axis))
    arrived = lax.all_to_all(pieces, axis, split_axis=0, concat_axis=0, tiled=True)
    return arrived.sum(axis=0)


def ancestry(parents):
    prop_count = parents.shape[1]
    indices = jnp.arange(prop_count, dtype=jnp.int32)
    linked = (parents[:, :, None] == indices[None, None, :]).astype(jnp.float32)
    linked = linked + (indices[:, None] == indices[None, :]).astype(jnp.float32)[None]
    for repeat in range(prop_count.bit_length()):
        linked = jnp.minimum(jnp.einsum("bij,bjk->bik", linked, linked), 1.0)
    return linked


def merge_pair(first_part, second_part):
    highest = jnp.maximum(first_part[0], second_part[0])
    scale_first = jnp.exp(first_part[0] - highest)
    scale_second = jnp.exp(second_part[0] - highest)
    seq_count, prop_count, head_count = highest.shape
    outer_first = (
        first_part[2].reshape(seq_count, prop_count, head_count, -1) * scale_first[..., None]
    )
    outer_second = (
        second_part[2].reshape(seq_count, prop_count, head_count, -1) * scale_second[..., None]
    )
    joined = (outer_first + outer_second).reshape(seq_count, prop_count, -1)
    return (highest, first_part[1] * scale_first + second_part[1] * scale_second, joined)


def local(
    tokens,
    norm_gain,
    w_query,
    w_key,
    w_value,
    w_forget,
    forget_bias,
    head_gain,
    w_out,
    cache_keys,
    cache_values,
    cache_gates,
    lengths,
    accepted,
    parents,
):
    seq_count, prop_count, model_width = tokens.shape
    span_rows = cache_keys.shape[1]
    head_count = cache_gates.shape[1]
    head_size = cache_keys.shape[2] // head_count
    scale = head_size ** (-0.5)
    start_pos = lax.axis_index(KV) * span_rows
    positions = start_pos + jnp.arange(span_rows, dtype=jnp.int32)
    valid_len = lengths + accepted
    flat_rows = tokens.reshape(seq_count * prop_count, model_width).astype(jnp.float32)
    normed = (
        flat_rows
        * lax.rsqrt(jnp.mean(flat_rows * flat_rows, axis=1, keepdims=True) + EPSILON)
        * norm_gain.astype(jnp.float32)
    ).astype(jnp.bfloat16)
    picked = (positions[None, :] == (valid_len - 1)[:, None]).astype(jnp.float32)
    last_part = jnp.sum(cache_gates * picked[:, None, :], axis=2)
    pieces = in_one_piece((w_query, w_key, w_value, w_forget), KV, 0, 1)
    query, fresh_keys, fresh_values, gate_pre = tuple(
        (jnp.dot(normed, piece, preferred_element_type=jnp.float32) for piece in pieces)
    )
    last_gate = one_axis_at_a_time(last_part, KV)
    query = query.astype(jnp.bfloat16).reshape(seq_count, prop_count, head_count, head_size)
    fresh_keys = fresh_keys.astype(jnp.bfloat16).reshape(
        seq_count, prop_count, head_count, head_size
    )
    fresh_values = fresh_values.astype(jnp.bfloat16).reshape(
        seq_count, prop_count, head_count, head_size
    )
    log_gate = jax.nn.log_sigmoid(gate_pre + forget_bias).reshape(seq_count, prop_count, head_count)
    link = ancestry(parents)
    climb = jnp.einsum("bia,bah->bih", link, log_gate)
    stored_keys = cache_keys.reshape(seq_count, span_rows, head_count, head_size)
    stored_values = cache_values.reshape(seq_count, span_rows, head_count, head_size)
    scores = (
        jnp.einsum("bphd,bchd->bphc", query, stored_keys, preferred_element_type=jnp.float32)
        * scale
    )
    scores = scores + (last_gate[:, None, :] + climb)[..., None] - cache_gates[:, None]
    seen = (positions[None, :] < valid_len[:, None])[:, None, None, :]
    highest = jnp.max(jnp.where(seen, scores, NEG_LARGE), axis=3)
    weights = jnp.where(seen, jnp.exp(scores - highest[..., None]), 0.0)
    normalizer = jnp.sum(weights, axis=3)
    weighted = jnp.einsum(
        "bphc,bchd->bphd",
        weights.astype(jnp.bfloat16),
        stored_values,
        preferred_element_type=jnp.float32,
    )
    highest, normalizer, weighted = merged_by_axis(
        (highest, normalizer, weighted.reshape(seq_count, prop_count, head_count * head_size)),
        KV,
        merge_pair,
    )
    near_scores = (
        jnp.einsum("bphd,bahd->bpha", query, fresh_keys, preferred_element_type=jnp.float32) * scale
    )
    near_scores = near_scores + climb[..., None] - jnp.transpose(climb, (0, 2, 1))[:, None]
    linked = (link > 0.5)[:, :, None, :]
    near_high = jnp.max(jnp.where(linked, near_scores, NEG_LARGE), axis=3)
    overall = jnp.maximum(highest, near_high)
    carried = jnp.exp(highest - overall)
    near_weights = jnp.where(linked, jnp.exp(near_scores - overall[..., None]), 0.0)
    normalizer = normalizer * carried + jnp.sum(near_weights, axis=3)
    attended = weighted.reshape(seq_count, prop_count, head_count, head_size) * carried[..., None]
    attended = attended + jnp.einsum(
        "bpha,bahd->bphd",
        near_weights.astype(jnp.bfloat16),
        fresh_values,
        preferred_element_type=jnp.float32,
    )
    attended = attended / normalizer[..., None]
    gain_rows = head_gain.astype(jnp.float32).reshape(head_count, head_size)
    heads_out = (
        (
            attended
            * lax.rsqrt(jnp.mean(attended * attended, axis=3, keepdims=True) + EPSILON)
            * gain_rows
        )
        .astype(jnp.bfloat16)
        .reshape(seq_count * prop_count, head_count * head_size)
    )
    partial_sum = jnp.dot(heads_out, w_out, preferred_element_type=jnp.float32)
    summed = sent_and_summed(partial_sum, "tp", 1)
    mixed = summed.reshape(seq_count, prop_count, -1)
    offsets = positions[None, :, None] - valid_len[:, None, None]
    placed = offsets == jnp.arange(prop_count, dtype=jnp.int32)[None, None, :]
    landed = jnp.any(placed, axis=2)
    placed_low = placed.astype(jnp.bfloat16)
    written_keys = jnp.einsum(
        "bcj,bjx->bcx",
        placed_low,
        fresh_keys.reshape(seq_count, prop_count, -1),
        preferred_element_type=jnp.float32,
    ).astype(jnp.bfloat16)
    written_values = jnp.einsum(
        "bcj,bjx->bcx",
        placed_low,
        fresh_values.reshape(seq_count, prop_count, -1),
        preferred_element_type=jnp.float32,
    ).astype(jnp.bfloat16)
    keys_out = jnp.where(landed[..., None], written_keys, cache_keys)
    values_out = jnp.where(landed[..., None], written_values, cache_values)
    new_gates = last_gate[:, :, None] + jnp.transpose(climb, (0, 2, 1))
    written_gates = jnp.einsum("bcj,bhj->bhc", placed.astype(jnp.float32), new_gates)
    gates_out = jnp.where(landed[:, None, :], written_gates, cache_gates)
    return (mixed, keys_out, values_out, gates_out)


def solution(mesh):
    torus = Mesh(
        mesh.devices.reshape(mesh.shape["dp"], 16, 4, mesh.shape["tp"]),
        ("dp", "kv_0", "kv_1", "tp"),
    )
    return jax.shard_map(
        local,
        mesh=torus,
        in_specs=(
            P("dp", None, None),
            P(),
            P(KV, "tp"),
            P(KV, "tp"),
            P(KV, "tp"),
            P(KV, "tp"),
            P("tp"),
            P("tp"),
            P("tp", KV),
            P("dp", KV, "tp"),
            P("dp", KV, "tp"),
            P("dp", "tp", KV),
            P("dp"),
            P("dp"),
            P("dp", None),
        ),
        out_specs=(P("dp", None, KV_TP), P("dp", KV, "tp"), P("dp", KV, "tp"), P("dp", "tp", KV)),
        check_vma=False,
    )
```

profile of v0, /device:TPU:1, one launch (start us, length us, event | category | flops | bytes accessed | tf_op | source)
XLA Modules:
  0.0 345.5 jit_solution(17081064558434147819)
XLA Ops:
  8.2 1.4 pad_maximum_fusion
  11.6 2.3 copy.57
  15.3 30.6 %psum.14 = f32[4,8]{1,0:T(4,128)S(1)} all-reduce(f32[4,8]{1,0:T(4,128)S(1)} %multiply_reduce_fusion.2), channel_id=1, replica_groups=mesh['dp'=4,'kv_0'=16,'kv_1'=4,'tp'=2] {'kv_0'}, use_global_device_ids=true, to_apply=%region_2.0 | all-reduce | flops 32 | bytes 256 | tf_op jit(solution)/shard_map/psum | solution.py:22
  45.8 9.1 %psum.15 = f32[4,8]{1,0:T(4,128)S(1)} all-reduce(f32[4,8]{1,0:T(4,128)S(1)} %psum.14), channel_id=1, replica_groups=mesh['dp'=4,'kv_0'=16,'kv_1'=4,'tp'=2] {'kv_1'}, use_global_device_ids=true, to_apply=%region_3.0 | all-reduce | flops 32 | bytes 256 | tf_op jit(solution)/shard_map/psum | solution.py:22
  56.5 104.4 %all-gather.7.cloned.1.call-done = bf16[2048,1544]{1,0:T(8,128)(2,1)} async-done(((bf16[32,1544]{1,0:T(8,128)(2,1)}), bf16[2048,1544]{1,0:T(8,128)(2,1)}) %all-gather.7.cloned.1.call-update) | async-done | bytes 6324240 | tf_op jit(solution)/shard_map/all_gather | solution.py:16
  162.3 2.1 fusion.16
  165.3 1.6 select_reduce_fusion
  167.6 1.6 fusion.28
  170.6 1.5 reshape.1556
  174.6 1.5 reshape.1554
  180.0 1.4 maximum_bitcast_fusion
  183.8 2.1 fusion.19
  186.1 2.1 fusion.22
  189.8 1.6 select_reduce_fusion.1
  191.4 1.5 fusion.6
  192.9 1.5 fusion.7
  194.4 57.1 %all-gather.9.cloned.1.call-done = f32[16,100,512]{2,1,0:T(8,128)} async-done(((f32[1,100,512]{2,1,0:T(8,128)}), f32[16,100,512]{2,1,0:T(8,128)}) %all-gather.9.cloned.1.call-update) | async-done | bytes 3276816 | tf_op jit(solution)/shard_map/all_gather | solution.py:34
  280.8 2.0 mul.671
  282.7 1.7 mul.664
  284.5 1.8 mul.665
  286.3 1.7 mul.667
  288.0 1.8 mul.668
  289.8 1.7 mul.658
  291.5 1.8 mul.659
  293.3 1.7 mul.652
  295.1 1.8 mul.653
  297.8 2.0 mul.656
  300.7 1.8 mul.647
  302.5 3.8 %fusion.45 = f32[96,512]{1,0:T(8,128)S(1)} fusion(f32[96,512]{1,0:T(8,128)} %mul.731, f32[16,100,512]{2,1,0:T(8,128)S(1)} %copy-done.3, f32[96,512]{1,0:T(8,128)} %mul.728, f32[96,512]{1,0:T(8,128)} %mul.725, f32[96,512]{1,0:T(8,128)} %mul.722, f32[96,512]{1,0:T(8,128)} %mul.719, f32[96,512]{1,0:T(8,128)} %mul.716, f32[96,512]{1,0:T(8,128)} %mul.713, ...), kind=kLoop, calls=%fused_computation.66 | loop fusion | flops 2211840 | bytes 9240576 | tf_op jit(solution)/shard_map/add | solution.py:84
  306.4 11.0 %all-gather.3 = f32[4,100,512]{2,1,0:T(8,128)S(1)} all-gather(f32[1,100,512]{2,1,0:T(8,128)S(1)} %maximum_bitcast_fusion.1), channel_id=3, replica_groups=mesh['dp'=4,'kv_0'=16,'kv_1'=4,'tp'=2] {'kv_1'}, dimensions={0}, use_global_device_ids=true | all-gather | bytes 1024000 | tf_op jit(solution)/shard_map/all_gather | solution.py:34
  319.6 1.7 multiply_reduce_fusion.1
  321.9 16.0 %all_to_all.5 = f32[2,96,16]{1,2,0:T(8,128)S(1)} all-to-all(f32[2,96,16]{1,2,0:T(8,128)S(1)} %convolution_bitcast_fusion.2), channel_id=1, replica_groups=mesh['dp'=4,'kv_0'=16,'kv_1'=4,'tp'=2] {'tp'}, dimensions={0} | all-to-all | bytes 24576 | tf_op jit(solution)/shard_map/all_to_all | solution.py:59
  (201 shorter events, 54.9 us)
Async XLA Ops:
  7.2 314.6 %copy-start = (bf16[512,32]{0,1:T(8,128)(2,1)S(1)}, bf16[512,32]{0,1:T(8,128)(2,1)}, u32[]{:S(2)}) copy-start(bf16[512,32]{0,1:T(8,128)(2,1)} %param.23) | copy-start | bytes 98308
  7.2 49.1 %copy-start.4 = (bf16[4,24,2048]{2,1,0:T(8,128)(2,1)S(1)}, bf16[4,24,2048]{2,1,0:T(8,128)(2,1)}, u32[]{:S(2)}) copy-start(bf16[4,24,2048]{2,1,0:T(8,128)(2,1)} %param.15) | copy-start | bytes 1179652
  7.2 6.7 %copy-start.2 = (bf16[4,256,512]{2,1,0:T(8,128)(2,1)S(1)}, bf16[4,256,512]{2,1,0:T(8,128)(2,1)}, u32[]{:S(2)}) copy-start(bf16[4,256,512]{2,1,0:T(8,128)(2,1)} %param.25) | copy-start | bytes 3145732
  7.2 7.2 %copy-start.18 = (s32[4]{0:T(128)S(1)}, s32[4]{0:T(128)}, u32[]{:S(2)}) copy-start(s32[4]{0:T(128)} %param.28) | copy-start | bytes 52
  7.2 7.2 %copy-start.17 = (s32[4]{0:T(128)S(1)}, s32[4]{0:T(128)}, u32[]{:S(2)}) copy-start(s32[4]{0:T(128)} %param.27) | copy-start | bytes 52
  7.2 7.9 %copy-start.6 = (f32[4,8,256]{2,1,0:T(8,128)S(1)}, f32[4,8,256]{2,1,0:T(8,128)}, u32[]{:S(2)}) copy-start(f32[4,8,256]{2,1,0:T(8,128)} %param.26) | copy-start | bytes 98308
  7.2 47.6 %copy-start.19 = (s32[4,24]{1,0:T(4,128)S(1)}, s32[4,24]{1,0:T(4,128)}, u32[]{:S(2)}) copy-start(s32[4,24]{1,0:T(4,128)} %param.29) | copy-start | bytes 1156
  7.2 153.6 %copy-start.16 = (f32[8]{0:T(128)S(1)}, f32[8]{0:T(128)}, u32[]{:S(2)}) copy-start(f32[8]{0:T(128)} %param.21) | copy-start | bytes 100
  7.3 153.6 %all-gather.7.cloned.1.call-start = ((), (), s32[]{:S(2)}) async-start(), calls=%async_computation.1 | async-start | bytes 6922240 | tf_op jit(solution)/shard_map/all_gather | solution.py:16
  9.6 241.9 %all-gather.9.cloned.1.call-start = ((), (), s32[]{:S(2)}) async-start(), calls=%async_computation.2 | async-start | bytes 3620864 | tf_op jit(solution)/shard_map/all_gather | solution.py:34
  14.5 147.8 %copy-start.15 = (s32[256]{0:T(256)}, s32[256]{0:T(256)S(1)}, u32[]{:S(2)}) copy-start(s32[256]{0:T(256)S(1)} %iota_add_fusion) | copy-start | bytes 3076
  14.5 0.7 copy-start.14
  54.9 110.4 %copy-start.9 = (f32[4,8]{1,0:T(4,128)}, f32[4,8]{1,0:T(4,128)S(1)}, u32[]{:S(2)}) copy-start(f32[4,8]{1,0:T(4,128)S(1)} %psum.15) | copy-start | bytes 388
  181.5 7.6 %copy-start.8 = (f32[4,24,8]{1,2,0:T(8,128)S(1)}, f32[4,24,8]{1,2,0:T(8,128)}, u32[]{:S(2)}) copy-start(f32[4,24,8]{1,2,0:T(8,128)} %get-tuple-element.142) | copy-start | bytes 9220
  181.5 7.6 %copy-start.10 = (f32[4,8]{1,0:T(4,128)S(1)}, f32[4,8]{1,0:T(4,128)}, u32[]{:S(2)}) copy-start(f32[4,8]{1,0:T(4,128)} %copy-done.9) | copy-start | bytes 388
  183.8 7.6 %copy-start.1 = (bf16[4,256,512]{2,1,0:T(8,128)(2,1)S(1)}, bf16[4,256,512]{2,1,0:T(8,128)(2,1)}, u32[]{:S(2)}) copy-start(bf16[4,256,512]{2,1,0:T(8,128)(2,1)} %param.24) | copy-start | bytes 3145732
  280.8 21.7 %copy-start.3 = (f32[16,100,512]{2,1,0:T(8,128)S(1)}, f32[16,100,512]{2,1,0:T(8,128)}, u32[]{:S(2)}) copy-start(f32[16,100,512]{2,1,0:T(8,128)} %all-gather.9.cloned.1.call-done) | copy-start | bytes 9830404
  302.5 3.8 %copy-start.11 = (f32[2,512]{1,0:T(2,128)S(1)}, f32[2,512]{1,0:T(2,128)}, u32[]{:S(2)}) copy-start(f32[2,512]{1,0:T(2,128)} %reshape.1561) | copy-start | bytes 12292
  302.5 3.8 %copy-start.12 = (f32[2,512]{1,0:T(2,128)S(1)}, f32[2,512]{1,0:T(2,128)}, u32[]{:S(2)}) copy-start(f32[2,512]{1,0:T(2,128)} %reshape.1559) | copy-start | bytes 12292
  306.3 13.1 %copy-start.13 = (f32[4,24,8]{1,2,0:T(8,128)S(1)}, f32[4,24,8]{1,2,0:T(8,128)}, u32[]{:S(2)}) copy-start(f32[4,24,8]{1,2,0:T(8,128)} %get-tuple-element.147) | copy-start | bytes 9220
  306.4 13.1 %copy-start.5 = (f32[4,24,8,24]{1,3,2,0:T(8,128)S(1)}, f32[4,24,8,24]{1,3,2,0:T(8,128)}, u32[]{:S(2)}) copy-start(f32[4,24,8,24]{1,3,2,0:T(8,128)} %get-tuple-element.148) | copy-start | bytes 221188
  306.4 13.2 %copy-start.7 = (bf16[4,24,8,64]{3,2,1,0:T(8,128)(2,1)S(1)}, bf16[4,24,8,64]{3,2,1,0:T(8,128)(2,1)}, u32[]{:S(2)}) copy-start(bf16[4,24,8,64]{3,2,1,0:T(8,128)(2,1)} %reshape.1564) | copy-start | bytes 294916
Sparse Core Ops, SparseCore 0:
  11.6 149.2 all-gather.6
  181.6 69.8 all-gather.8
where the time goes:
time: 347 us; the launch traced here: 345 us
  waiting for transfers between devices  162 us (47%)
  local copies, waits for them, and re-layouts  68.7 us (20%)
  blocking collectives  66.7 us (19%)
  matrix products  19.6 us (6%)
  between operations  14.9 us (4%)
  other arithmetic  13.9 us (4%)
    all_gather x1, waiting for transfers between devices, in_one_piece(): whole = lax.all_gather(both, axis, axis=dim, tiled=True)  104 us
    all_gather x1, waiting for transfers between devices, collected_together(): both, at, found = (lax.all_gather(jnp.concatenate(lines), axis), 0, {})  57.1 us
    psum x2, blocking collectives, one_axis_at_a_time(): array = lax.psum(array, axis)  39.6 us
    mul x30, local copies, waits for them, and re-layouts, merge_pair(): second_part[2].reshape(seq_count, prop_count, head_count, -1)  26 us
    mul x30, local copies, waits for them, and re-layouts, merge_pair(): first_part[2].reshape(seq_count, prop_count, head_count, -1)  19.1 us
    all_to_all x1, blocking collectives, sent_and_summed(): lax.all_to_all(pieces, axis, split_axis=0, concat_axis=0, tiled=True)  16 us
    all_gather x1, blocking collectives, collected_together(): both, at, found = (lax.all_gather(jnp.concatenate(lines), axis), 0, {})  11 us
    dot_general x4, matrix products, local(): jnp.dot(normed, piece, preferred_element_type=jnp.float32)  7.6 us
  transfers between devices with their start and end apart: 2, of which 2 were waited for; matrix products, arithmetic and copies ran while one was open for 6% of the time, Pallas kernels for 0%

commit v1 on v0

--- a/solution.py
+++ b/solution.py
@@ -19,7 +19,8 @@
 
 def one_axis_at_a_time(array, axes):
     for axis in axes:
-        array = lax.psum(array, axis)
+        _launch_sheet = lambda chunk, axis_name: jnp.sum(lax.all_gather(chunk, axis_name), 0)
+        array = _launch_sheet(array, axis)
     return array
 
 

time: 347 us -> 347 us (level)
    psum x2 -> x0, blocking collectives: 39.6 us -> none  [one_axis_at_a_time(): array = lax.psum(array, axis)]
    all_gather x0 -> x2, blocking collectives: none -> 39.4 us  [one_axis_at_a_time(): lax.all_gather(chunk, axis_name)]
where the time goes in v1:
time: 347 us; the launch traced here: 345 us
  waiting for transfers between devices  160 us (46%)
  local copies, waits for them, and re-layouts  68.7 us (20%)
  blocking collectives  66.4 us (19%)
  matrix products  19.6 us (6%)
  other arithmetic  15.4 us (4%)
  between operations  14.9 us (4%)
    all_gather x1, waiting for transfers between devices, in_one_piece(): whole = lax.all_gather(both, axis, axis=dim, tiled=True)  103 us
    all_gather x1, waiting for transfers between devices, collected_together(): both, at, found = (lax.all_gather(jnp.concatenate(lines), axis), 0, {})  57.1 us
    all_gather x2, blocking collectives, one_axis_at_a_time(): lax.all_gather(chunk, axis_name)  39.4 us
    mul x30, local copies, waits for them, and re-layouts, merge_pair(): second_part[2].reshape(seq_count, prop_count, head_count, -1)  26 us
    mul x30, local copies, waits for them, and re-layouts, merge_pair(): first_part[2].reshape(seq_count, prop_count, head_count, -1)  19.1 us
    all_to_all x1, blocking collectives, sent_and_summed(): lax.all_to_all(pieces, axis, split_axis=0, concat_axis=0, tiled=True)  16 us
    all_gather x1, blocking collectives, collected_together(): both, at, found = (lax.all_gather(jnp.concatenate(lines), axis), 0, {})  11 us
    dot_general x4, matrix products, local(): jnp.dot(normed, piece, preferred_element_type=jnp.float32)  7.59 us
  transfers between devices with their start and end apart: 2, of which 2 were waited for; matrix products, arithmetic and copies ran while one was open for 6% of the time, Pallas kernels for 0%

profile of v1, /device:TPU:1, one launch (start us, length us, event | category | flops | bytes accessed | tf_op | source)
XLA Modules:
  0.0 345.5 jit_solution(4843076343569136830)
XLA Ops:
  8.1 1.4 pad_maximum_fusion
  13.8 29.4 %all-gather.4 = f32[16,4,8]{2,1,0:T(4,128)S(1)} all-gather(f32[1,4,8]{2,1,0:T(4,128)S(1)} %bitcast.303), channel_id=2, replica_groups=mesh['dp'=4,'kv_0'=16,'kv_1'=4,'tp'=2] {'kv_0'}, dimensions={0}, use_global_device_ids=true | all-gather | bytes 2176 | tf_op jit(solution)/shard_map/all_gather | solution.py:22
  43.3 9.9 %all-gather.5 = f32[4,4,8]{2,1,0:T(4,128)S(1)} all-gather(f32[1,4,8]{2,1,0:T(4,128)S(1)} %bitcast.304), channel_id=3, replica_groups=mesh['dp'=4,'kv_0'=16,'kv_1'=4,'tp'=2] {'kv_1'}, dimensions={0}, use_global_device_ids=true | all-gather | bytes 640 | tf_op jit(solution)/shard_map/all_gather | solution.py:22
  53.2 2.3 copy.57
  57.6 103.2 %all-gather.11.cloned.1.call-done = bf16[2048,1544]{1,0:T(8,128)(2,1)} async-done(((bf16[32,1544]{1,0:T(8,128)(2,1)}), bf16[2048,1544]{1,0:T(8,128)(2,1)}) %all-gather.11.cloned.1.call-update) | async-done | bytes 6324240 | tf_op jit(solution)/shard_map/all_gather | solution.py:16
  162.3 2.1 fusion.16
  165.2 1.6 select_reduce_fusion
  167.6 1.6 fusion.28
  170.6 1.5 reshape.1556
  174.6 1.5 reshape.1554
  180.0 1.4 maximum_bitcast_fusion
  183.8 2.1 fusion.19
  186.1 2.1 fusion.22
  189.8 1.6 select_reduce_fusion.1
  191.4 1.5 fusion.6
  192.9 1.5 fusion.7
  194.4 57.1 %all-gather.13.cloned.1.call-done = f32[16,100,512]{2,1,0:T(8,128)} async-done(((f32[1,100,512]{2,1,0:T(8,128)}), f32[16,100,512]{2,1,0:T(8,128)}) %all-gather.13.cloned.1.call-update) | async-done | bytes 3276816 | tf_op jit(solution)/shard_map/all_gather | solution.py:35
  280.8 2.0 mul.671
  282.7 1.7 mul.664
  284.5 1.8 mul.665
  286.3 1.7 mul.667
  288.0 1.8 mul.668
  289.8 1.7 mul.658
  291.5 1.8 mul.659
  293.3 1.7 mul.652
  295.0 1.8 mul.653
  297.8 2.0 mul.656
  300.7 1.8 mul.647
  302.5 3.8 %fusion.45 = f32[96,512]{1,0:T(8,128)S(1)} fusion(f32[96,512]{1,0:T(8,128)} %mul.731, f32[16,100,512]{2,1,0:T(8,128)S(1)} %copy-done.3, f32[96,512]{1,0:T(8,128)} %mul.728, f32[96,512]{1,0:T(8,128)} %mul.725, f32[96,512]{1,0:T(8,128)} %mul.722, f32[96,512]{1,0:T(8,128)} %mul.719, f32[96,512]{1,0:T(8,128)} %mul.716, f32[96,512]{1,0:T(8,128)} %mul.713, ...), kind=kLoop, calls=%fused_computation.66 | loop fusion | flops 2211840 | bytes 9240576 | tf_op jit(solution)/shard_map/add | solution.py:85
  306.4 11.0 %all-gather.7 = f32[4,100,512]{2,1,0:T(8,128)S(1)} all-gather(f32[1,100,512]{2,1,0:T(8,128)S(1)} %maximum_bitcast_fusion.1), channel_id=5, replica_groups=mesh['dp'=4,'kv_0'=16,'kv_1'=4,'tp'=2] {'kv_1'}, dimensions={0}, use_global_device_ids=true | all-gather | bytes 1024000 | tf_op jit(solution)/shard_map/all_gather | solution.py:35
  319.6 1.7 multiply_reduce_fusion.1
  321.9 16.0 %all_to_all.5 = f32[2,96,16]{1,2,0:T(8,128)S(1)} all-to-all(f32[2,96,16]{1,2,0:T(8,128)S(1)} %convolution_bitcast_fusion.2), channel_id=1, replica_groups=mesh['dp'=4,'kv_0'=16,'kv_1'=4,'tp'=2] {'tp'}, dimensions={0} | all-to-all | bytes 24576 | tf_op jit(solution)/shard_map/all_to_all | solution.py:60
  (199 shorter events, 56.3 us)
Async XLA Ops:
  7.2 314.6 %copy-start = (bf16[512,32]{0,1:T(8,128)(2,1)S(1)}, bf16[512,32]{0,1:T(8,128)(2,1)}, u32[]{:S(2)}) copy-start(bf16[512,32]{0,1:T(8,128)(2,1)} %param.23) | copy-start | bytes 98308
  7.2 50.2 %copy-start.4 = (bf16[4,24,2048]{2,1,0:T(8,128)(2,1)S(1)}, bf16[4,24,2048]{2,1,0:T(8,128)(2,1)}, u32[]{:S(2)}) copy-start(bf16[4,24,2048]{2,1,0:T(8,128)(2,1)} %param.15) | copy-start | bytes 1179652
  7.2 48.3 %copy-start.2 = (bf16[4,256,512]{2,1,0:T(8,128)(2,1)S(1)}, bf16[4,256,512]{2,1,0:T(8,128)(2,1)}, u32[]{:S(2)}) copy-start(bf16[4,256,512]{2,1,0:T(8,128)(2,1)} %param.25) | copy-start | bytes 3145732
  7.2 48.8 %copy-start.17 = (s32[4,24]{1,0:T(4,128)S(1)}, s32[4,24]{1,0:T(4,128)}, u32[]{:S(2)}) copy-start(s32[4,24]{1,0:T(4,128)} %param.29) | copy-start | bytes 1156
  7.2 153.6 %copy-start.16 = (f32[8]{0:T(128)S(1)}, f32[8]{0:T(128)}, u32[]{:S(2)}) copy-start(f32[8]{0:T(128)} %param.21) | copy-start | bytes 100
  7.2 153.6 %all-gather.11.cloned.1.call-start = ((), (), s32[]{:S(2)}) async-start(), calls=%async_computation.1 | async-start | bytes 6922240 | tf_op jit(solution)/shard_map/all_gather | solution.py:16
  9.6 241.9 %all-gather.13.cloned.1.call-start = ((), (), s32[]{:S(2)}) async-start(), calls=%async_computation.2 | async-start | bytes 3620864 | tf_op jit(solution)/shard_map/all_gather | solution.py:35
  11.6 2.2 copy-start.15
  12.3 0.7 copy-start.14
  53.2 111.3 %copy-start.9 = (f32[4,8]{1,0:T(4,128)}, f32[4,8]{1,0:T(4,128)S(1)}, u32[]{:S(2)}) copy-start(f32[4,8]{1,0:T(4,128)S(1)} %reduce_sum.75) | copy-start | bytes 388
  55.5 109.8 %copy-start.6 = (f32[4,8,256]{2,1,0:T(8,128)S(1)}, f32[4,8,256]{2,1,0:T(8,128)}, u32[]{:S(2)}) copy-start(f32[4,8,256]{2,1,0:T(8,128)} %param.26) | copy-start | bytes 98308
  181.4 7.6 %copy-start.8 = (f32[4,24,8]{1,2,0:T(8,128)S(1)}, f32[4,24,8]{1,2,0:T(8,128)}, u32[]{:S(2)}) copy-start(f32[4,24,8]{1,2,0:T(8,128)} %get-tuple-element.142) | copy-start | bytes 9220
  181.4 7.6 %copy-start.10 = (f32[4,8]{1,0:T(4,128)S(1)}, f32[4,8]{1,0:T(4,128)}, u32[]{:S(2)}) copy-start(f32[4,8]{1,0:T(4,128)} %copy-done.9) | copy-start | bytes 388
  183.8 7.6 %copy-start.1 = (bf16[4,256,512]{2,1,0:T(8,128)(2,1)S(1)}, bf16[4,256,512]{2,1,0:T(8,128)(2,1)}, u32[]{:S(2)}) copy-start(bf16[4,256,512]{2,1,0:T(8,128)(2,1)} %param.24) | copy-start | bytes 3145732
  280.8 21.7 %copy-start.3 = (f32[16,100,512]{2,1,0:T(8,128)S(1)}, f32[16,100,512]{2,1,0:T(8,128)}, u32[]{:S(2)}) copy-start(f32[16,100,512]{2,1,0:T(8,128)} %all-gather.13.cloned.1.call-done) | copy-start | bytes 9830404
  302.5 3.8 %copy-start.11 = (f32[2,512]{1,0:T(2,128)S(1)}, f32[2,512]{1,0:T(2,128)}, u32[]{:S(2)}) copy-start(f32[2,512]{1,0:T(2,128)} %reshape.1561) | copy-start | bytes 12292
  302.5 3.8 %copy-start.12 = (f32[2,512]{1,0:T(2,128)S(1)}, f32[2,512]{1,0:T(2,128)}, u32[]{:S(2)}) copy-start(f32[2,512]{1,0:T(2,128)} %reshape.1559) | copy-start | bytes 12292
  306.3 13.1 %copy-start.13 = (f32[4,24,8]{1,2,0:T(8,128)S(1)}, f32[4,24,8]{1,2,0:T(8,128)}, u32[]{:S(2)}) copy-start(f32[4,24,8]{1,2,0:T(8,128)} %get-tuple-element.147) | copy-start | bytes 9220
  306.4 13.1 %copy-start.5 = (f32[4,24,8,24]{1,3,2,0:T(8,128)S(1)}, f32[4,24,8,24]{1,3,2,0:T(8,128)}, u32[]{:S(2)}) copy-start(f32[4,24,8,24]{1,3,2,0:T(8,128)} %get-tuple-element.148) | copy-start | bytes 221188
  306.4 13.2 %copy-start.7 = (bf16[4,24,8,64]{3,2,1,0:T(8,128)(2,1)S(1)}, bf16[4,24,8,64]{3,2,1,0:T(8,128)(2,1)}, u32[]{:S(2)}) copy-start(bf16[4,24,8,64]{3,2,1,0:T(8,128)(2,1)} %reshape.1564) | copy-start | bytes 294916
Sparse Core Ops, SparseCore 0:
  11.6 149.2 all-gather.10
  181.6 69.8 all-gather.12
